TPU v7x, 32 devices: a whole 2x2x4 slice. The times are simulated.
32 devices in a mesh: fs: 8 (over z, core), tp: 4 (over y, x).
Axes of the slice: x: 2, y: 2, z: 4, core: 2. Of those that a mesh axis runs over, the one named last changes fastest.
Arguments:
- late_input: bfloat16 [1024, 2048], P('fs'), may hold values from -6 to 6
- early_input: bfloat16 [1024, 2048], P('fs'), may hold values from -6 to 6
- early_mid: bfloat16 [1024, 2048], P('fs'), may hold values from -6 to 6
- cotangent: bfloat16 [1024, 2048], P('fs'), may hold values from -6 to 6
- gain_first: float32 [2048], replicated, may hold values from 0.1 to 1.9
- gain_second: float32 [2048], replicated, may hold values from 0.1 to 1.9
- gate_first: bfloat16 [2048, 2816], P('fs', 'tp'), may hold values from -0.125 to 0.125
- up_first: bfloat16 [2048, 2816], P('fs', 'tp'), may hold values from -0.125 to 0.125
- down_first: bfloat16 [2816, 2048], P('tp', 'fs'), may hold values from -0.109375 to 0.109375
- gate_second: bfloat16 [2048, 2816], P('fs', 'tp'), may hold values from -0.125 to 0.125
- up_second: bfloat16 [2048, 2816], P('fs', 'tp'), may hold values from -0.125 to 0.125
- down_second: bfloat16 [2816, 2048], P('tp', 'fs'), may hold values from -0.109375 to 0.109375
- sum_gate_first: float32 [2048, 2816], P('fs', 'tp'), may hold values from -128 to 128
- sum_up_first: float32 [2048, 2816], P('fs', 'tp'), may hold values from -128 to 128
- sum_down_first: float32 [2816, 2048], P('tp', 'fs'), may hold values from -128 to 128
- sum_gate_second: float32 [2048, 2816], P('fs', 'tp'), may hold values from -128 to 128
- sum_up_second: float32 [2048, 2816], P('fs', 'tp'), may hold values from -128 to 128
- sum_down_second: float32 [2816, 2048], P('tp', 'fs'), may hold values from -128 to 128
Outputs:
- late_mid: bfloat16 [1024, 2048], P('fs')
- late_out: bfloat16 [1024, 2048], P('fs')
- input_grad: bfloat16 [1024, 2048], P('fs')
- new_gate_first: float32 [2048, 2816], P('fs', 'tp')
- new_up_first: float32 [2048, 2816], P('fs', 'tp')
- new_down_first: float32 [2816, 2048], P('tp', 'fs')
- new_gate_second: float32 [2048, 2816], P('fs', 'tp')
- new_up_second: float32 [2048, 2816], P('fs', 'tp')
- new_down_second: float32 [2816, 2048], P('tp', 'fs')
All inputs are finite; a program needn't handle non-finite values.
Results may differ from a plain program's by a relative error of at most 0.015.
Values may be sent and summed in bfloat16 or wider, within the bound.
A program may use at most 128 MiB of HBM per device.

v0:
```python
import jax
import jax.numpy as jnp
from jax import lax
from jax.sharding import PartitionSpec as P

norm_eps = 1e-06


def normalize(values, gain_vector):
    widened = values.astype(jnp.float32)
    factor = lax.rsqrt(jnp.mean(widened * widened, axis=-1, keepdims=True) + norm_eps)
    normed = (widened * factor * gain_vector).astype(jnp.bfloat16)
    return (widened, factor, normed)


def block_forward(values, params):
    gain_vector, w_gate, w_up, w_down = params
    widened, factor, normed = normalize(values, gain_vector)
    gate_pre = jnp.dot(normed, w_gate, preferred_element_type=jnp.float32)
    up_pre = jnp.dot(normed, w_up, preferred_element_type=jnp.float32)
    hidden = (jax.nn.silu(gate_pre) * up_pre).astype(jnp.bfloat16)
    branch = lax.psum(
        jnp.dot(hidden, w_down, preferred_element_type=jnp.float32).astype(jnp.bfloat16), "tp"
    ).astype(jnp.float32)
    return (widened + 0.5 * branch).astype(jnp.bfloat16)


def block_backward(values, cotangent, params):
    gain_vector, w_gate, w_up, w_down = params
    widened, factor, normed = normalize(values, gain_vector)
    gate_pre = jnp.dot(normed, w_gate, preferred_element_type=jnp.float32)
    up_pre = jnp.dot(normed, w_up, preferred_element_type=jnp.float32)
    sigmoid_gate = jax.nn.sigmoid(gate_pre)
    activated = gate_pre * sigmoid_gate
    hidden = (activated * up_pre).astype(jnp.bfloat16)
    hidden_grad = 0.5 * jnp.einsum(
        "td,fd->tf", cotangent, w_down, preferred_element_type=jnp.float32
    )
    gate_grad = (
        hidden_grad * up_pre * sigmoid_gate * (1.0 + gate_pre * (1.0 - sigmoid_gate))
    ).astype(jnp.bfloat16)
    up_grad = (hidden_grad * activated).astype(jnp.bfloat16)
    partial_value = jnp.einsum("tf,df->td", gate_grad, w_gate, preferred_element_type=jnp.float32)
    partial_value = partial_value + jnp.einsum(
        "tf,df->td", up_grad, w_up, preferred_element_type=jnp.float32
    )
    normed_grad = lax.psum(partial_value.astype(jnp.bfloat16), "tp").astype(jnp.float32)
    scaled = normed_grad * gain_vector
    unit_rows = widened * factor
    rows_grad = cotangent.astype(jnp.float32) + factor * (
        scaled - unit_rows * jnp.mean(scaled * unit_rows, axis=-1, keepdims=True)
    )
    return (rows_grad, (normed, cotangent, gate_grad, up_grad, hidden))


def fold_pair(pieces, columns_in):
    return (
        jnp.einsum("td,tf->df", columns_in, pieces[0], preferred_element_type=jnp.float32),
        jnp.einsum("td,tf->df", columns_in, pieces[1], preferred_element_type=jnp.float32),
    )


def fold_block(pieces, columns_in, columns_out):
    paired = fold_pair(pieces[0:2], columns_in)
    return paired + (
        jnp.einsum("tf,td->fd", pieces[2], columns_out, preferred_element_type=jnp.float32),
    )


def per_device(
    late_input,
    early_input,
    early_mid,
    cotangent,
    gain_first,
    gain_second,
    gate_first,
    up_first,
    down_first,
    gate_second,
    up_second,
    down_second,
    sum_gate_first,
    sum_up_first,
    sum_down_first,
    sum_gate_second,
    sum_up_second,
    sum_down_second,
):
    rows_in = (
        lax.all_gather(gate_first, "fs", axis=0, tiled=True),
        lax.all_gather(up_first, "fs", axis=0, tiled=True),
        lax.all_gather(gate_second, "fs", axis=0, tiled=True),
        lax.all_gather(up_second, "fs", axis=0, tiled=True),
    )
    cols_out = (
        lax.all_gather(down_first, "fs", axis=1, tiled=True),
        lax.all_gather(down_second, "fs", axis=1, tiled=True),
    )
    first_params = (gain_first, rows_in[0], rows_in[1], cols_out[0])
    second_params = (gain_second, rows_in[2], rows_in[3], cols_out[1])
    late_mid = block_forward(late_input, first_params)
    late_out = block_forward(late_mid, second_params)

    def collect(saved_parts):
        normed, cotan_rows, gate_grad, up_grad, hidden = saved_parts
        columns_in, columns_out = (
            lax.all_to_all(normed, "fs", split_axis=1, concat_axis=0, tiled=True),
            lax.all_to_all(cotan_rows, "fs", split_axis=1, concat_axis=0, tiled=True),
        )
        result = fold_block(
            (
                lax.all_gather(gate_grad, "fs", axis=0, tiled=True),
                lax.all_gather(up_grad, "fs", axis=0, tiled=True),
                lax.all_gather(hidden, "fs", axis=0, tiled=True),
            ),
            columns_in,
            columns_out,
        )
        return (result[0], result[1], 0.5 * result[2])

    mid_grad, saved_second = block_backward(early_mid, cotangent, second_params)
    mid_grad = mid_grad.astype(jnp.bfloat16)
    grads_second = collect(saved_second)
    rows_grad, saved_first = block_backward(early_input, mid_grad, first_params)
    grads_first = collect(saved_first)
    return (
        late_mid,
        late_out,
        rows_grad.astype(jnp.bfloat16),
        sum_gate_first + grads_first[0],
        sum_up_first + grads_first[1],
        sum_down_first + grads_first[2],
        sum_gate_second + grads_second[0],
        sum_up_second + grads_second[1],
        sum_down_second + grads_second[2],
    )


def solution(mesh):
    in_specs = (
        P("fs", None),
        P("fs", None),
        P("fs", None),
        P("fs", None),
        P(),
        P(),
        P("fs", "tp"),
        P("fs", "tp"),
        P("tp", "fs"),
        P("fs", "tp"),
        P("fs", "tp"),
        P("tp", "fs"),
        P("fs", "tp"),
        P("fs", "tp"),
        P("tp", "fs"),
        P("fs", "tp"),
        P("fs", "tp"),
        P("tp", "fs"),
    )
    out_specs = (
        P("fs", None),
        P("fs", None),
        P("fs", None),
        P("fs", "tp"),
        P("fs", "tp"),
        P("tp", "fs"),
        P("fs", "tp"),
        P("fs", "tp"),
        P("tp", "fs"),
    )
    return jax.shard_map(
        per_device, mesh=mesh, in_specs=in_specs, out_specs=out_specs, check_vma=False
    )
```

profile of v0, /device:TPU:9, one launch (start us, length us, event | category | flops | bytes accessed | tf_op | source)
XLA Modules:
  0.0 554.4 jit_solution(9023970974551871583)
XLA Ops:
  13.0 33.9 %all-gather.19.cloned.1.call-done = bf16[2048,704]{0,1:T(8,128)(2,1)} async-done(((bf16[256,704]{0,1:T(8,128)(2,1)}), bf16[2048,704]{0,1:T(8,128)(2,1)}) %all-gather.19.cloned.1.call-update) | async-done | bytes 2883600 | tf_op jit(solution)/shard_map/all_gather | solution.py:93
  46.8 3.5 fusion.59
  50.3 33.4 %all-gather.23.cloned.1.call-done = bf16[704,2048]{1,0:T(8,128)(2,1)} async-done(((bf16[704,256]{1,0:T(8,128)(2,1)}), bf16[704,2048]{1,0:T(8,128)(2,1)}) %all-gather.23.cloned.1.call-update) | async-done | bytes 2883600 | tf_op jit(solution)/shard_map/all_gather | solution.py:98
  83.7 3.5 convolution_multiply_fusion.3
  87.2 33.4 %all-gather.13.cloned.1.call-done = bf16[2048,704]{0,1:T(8,128)(2,1)} async-done(((bf16[256,704]{0,1:T(8,128)(2,1)}), bf16[2048,704]{0,1:T(8,128)(2,1)}) %all-gather.13.cloned.1.call-update) | async-done | bytes 2883600 | tf_op jit(solution)/shard_map/all_gather | solution.py:91
  120.6 3.5 fusion.54
  124.1 33.2 %all-gather.21.cloned.1.call-done = bf16[2048,704]{0,1:T(8,128)(2,1)} async-done(((bf16[256,704]{0,1:T(8,128)(2,1)}), bf16[2048,704]{0,1:T(8,128)(2,1)}) %all-gather.21.cloned.1.call-update) | async-done | bytes 2883600 | tf_op jit(solution)/shard_map/all_gather | solution.py:94
  157.3 3.8 multiply_convert_fusion
  163.6 3.7 fusion
  167.3 26.7 %all-gather.15.cloned.1.call-done = bf16[2048,704]{0,1:T(8,128)(2,1)} async-done(((bf16[256,704]{0,1:T(8,128)(2,1)}), bf16[2048,704]{0,1:T(8,128)(2,1)}) %all-gather.15.cloned.1.call-update) | async-done | bytes 2883600 | tf_op jit(solution)/shard_map/all_gather | solution.py:92
  194.0 36.7 %all-gather.17.cloned.1.call-done = bf16[704,2048]{1,0:T(8,128)(2,1)} async-done(((bf16[704,256]{1,0:T(8,128)(2,1)}), bf16[704,2048]{1,0:T(8,128)(2,1)}) %all-gather.17.cloned.1.call-update) | async-done | bytes 2883600 | tf_op jit(solution)/shard_map/all_gather | solution.py:97
  230.7 6.0 %convolution_convert_fusion.1 = bf16[128,2048]{1,0:T(8,128)(2,1)} fusion(bf16[704,2048]{1,0:T(8,128)(2,1)} %all-gather.17.cloned.1.call-done, bf16[2048,704]{0,1:T(8,128)(2,1)} %all-gather.15.cloned.1.call-done, f32[128,704]{0,1:T(8,128)} %fusion.54, bf16[128,2048]{1,0:T(8,128)(2,1)} %param.18, f32[2048]{0:T(1024)S(1)} %copy-done.23, f32[128]{0:T(128)S(1)} %add_rsqrt_fusion.3), kind=kOutput, calls=%fused_computation.5 | convolution fusion | flops 740048896 | bytes 7184896 | tf_op jit(solution)/shard_map/dot_general | solution.py:23
  240.2 3.5 fusion.61
  243.7 44.7 %all-reduce.7.cloned.1.call-done = (bf16[128,2048]{1,0:T(8,128)(2,1)}, bf16[128,2048]{1,0:T(8,128)(2,1)}) async-done(((bf16[128,2048]{1,0:T(8,128)(2,1)}, bf16[128,2048]{1,0:T(8,128)(2,1)}), (bf16[128,2048]{1,0:T(8,128)(2,1)}, bf16[128,2048]{1,0:T(8,128)(2,1)})) %all-reduce.7.cloned.1.call-update) | async-done | bytes 1048592 | tf_op jit(solution)/shard_map/psum | solution.py:22
  296.0 3.6 fusion.62
  301.3 6.0 %convolution_convert_fusion = bf16[128,2048]{1,0:T(8,128)(2,1)} fusion(bf16[704,2048]{1,0:T(8,128)(2,1)} %all-gather.23.cloned.1.call-done, bf16[2048,704]{0,1:T(8,128)(2,1)} %all-gather.21.cloned.1.call-done, f32[128,704]{0,1:T(8,128)} %fusion.50, bf16[128,2048]{1,0:T(8,128)(2,1)S(1)} %get-tuple-element.14, f32[2048]{0:T(1024)S(1)} %copy-done.22, ...), kind=kOutput, calls=%fused_computation.4 | convolution fusion | flops 740048896 | bytes 7184896 | tf_op jit(solution)/shard_map/dot_general | solution.py:23
  315.5 5.7 %all-to-all-start.3 = ((bf16[128,8,256]{0,2,1:T(8,128)(2,1)}), bf16[128,8,256]{0,2,1:T(8,128)(2,1)S(1)}, u32[]{:S(2)}, u32[]{:S(2)}) async-start(bf16[128,8,256]{0,2,1:T(8,128)(2,1)} %bitcast.8), calls=%async_computation.3 | async-start | bytes 1048576 | tf_op jit(solution)/shard_map/all_to_all | solution.py:109
  322.0 11.0 %all-to-all-done.3 = bf16[128,8,256]{0,2,1:T(8,128)(2,1)S(1)} async-done(((bf16[128,8,256]{0,2,1:T(8,128)(2,1)}), bf16[128,8,256]{0,2,1:T(8,128)(2,1)S(1)}, u32[]{:S(2)}, u32[]{:S(2)}) %all-to-all-start.3) | async-done | bytes 524320 | tf_op jit(solution)/shard_map/all_to_all | solution.py:109
  333.0 6.9 %all-to-all-start.2 = ((bf16[128,8,256]{2,0,1:T(8,128)(2,1)}), bf16[128,8,256]{2,0,1:T(8,128)(2,1)S(1)}, u32[]{:S(2)}, u32[]{:S(2)}) async-start(bf16[128,8,256]{2,0,1:T(8,128)(2,1)} %bitcast.59), calls=%async_computation.2 | async-start | bytes 1048576 | tf_op jit(solution)/shard_map/all_to_all | solution.py:108
  341.8 20.8 %all-reduce.5.cloned.1.call-done = (bf16[128,2048]{1,0:T(8,128)(2,1)}, bf16[128,2048]{1,0:T(8,128)(2,1)}) async-done(((bf16[128,2048]{1,0:T(8,128)(2,1)}, bf16[128,2048]{1,0:T(8,128)(2,1)}), (bf16[128,2048]{1,0:T(8,128)(2,1)}, bf16[128,2048]{1,0:T(8,128)(2,1)})) %all-reduce.5.cloned.1.call-update) | async-done | bytes 1048592 | tf_op jit(solution)/shard_map/psum | solution.py:22
  366.3 5.6 %all-to-all-start = ((bf16[128,8,256]{2,0,1:T(8,128)(2,1)}), bf16[128,8,256]{2,0,1:T(8,128)(2,1)S(1)}, u32[]{:S(2)}, u32[]{:S(2)}) async-start(bf16[128,8,256]{2,0,1:T(8,128)(2,1)} %bitcast.61), calls=%async_computation | async-start | bytes 1048576 | tf_op jit(solution)/shard_map/all_to_all | solution.py:108
  373.9 27.7 %all-gather.33.cloned.1.call-done = bf16[1024,704]{0,1:T(8,128)(2,1)} async-done(((bf16[128,704]{0,1:T(8,128)(2,1)}), bf16[1024,704]{0,1:T(8,128)(2,1)}) %all-gather.33.cloned.1.call-update) | async-done | bytes 1441808 | tf_op jit(solution)/shard_map/all_gather | solution.py:114
  404.4 25.2 %all-gather.31.cloned.1.call-done = bf16[1024,704]{0,1:T(8,128)(2,1)} async-done(((bf16[128,704]{0,1:T(8,128)(2,1)}), bf16[1024,704]{0,1:T(8,128)(2,1)}) %all-gather.31.cloned.1.call-update) | async-done | bytes 1441808 | tf_op jit(solution)/shard_map/all_gather | solution.py:113
  429.6 2.9 convolution_add_fusion.3
  432.6 3.6 all-to-all-start.1
  436.2 29.4 %all-gather.35.cloned.1.call-done = bf16[1024,704]{0,1:T(8,128)(2,1)} async-done(((bf16[128,704]{0,1:T(8,128)(2,1)}), bf16[1024,704]{0,1:T(8,128)(2,1)}) %all-gather.35.cloned.1.call-update) | async-done | bytes 1441808 | tf_op jit(solution)/shard_map/all_gather | solution.py:115
  465.5 2.8 fusion.8
  468.3 23.7 %all-gather.27.cloned.1.call-done = bf16[1024,704]{0,1:T(8,128)(2,1)} async-done(((bf16[128,704]{0,1:T(8,128)(2,1)}), bf16[1024,704]{0,1:T(8,128)(2,1)}) %all-gather.27.cloned.1.call-update) | async-done | bytes 1441808 | tf_op jit(solution)/shard_map/all_gather | solution.py:114
  492.0 2.8 convolution_add_fusion.4
  494.9 23.8 %all-gather.25.cloned.1.call-done = bf16[1024,704]{0,1:T(8,128)(2,1)} async-done(((bf16[128,704]{0,1:T(8,128)(2,1)}), bf16[1024,704]{0,1:T(8,128)(2,1)}) %all-gather.25.cloned.1.call-update) | async-done | bytes 1441808 | tf_op jit(solution)/shard_map/all_gather | solution.py:113
  521.4 23.7 %all-gather.29.cloned.1.call-done = bf16[1024,704]{0,1:T(8,128)(2,1)} async-done(((bf16[128,704]{0,1:T(8,128)(2,1)}), bf16[1024,704]{0,1:T(8,128)(2,1)}) %all-gather.29.cloned.1.call-update) | async-done | bytes 1441808 | tf_op jit(solution)/shard_map/all_gather | solution.py:115
  545.1 2.8 fusion.9
  (108 shorter events, 43.0 us)
Async XLA Ops:
  7.2 39.6 %all-gather.19.cloned.1.call-start = ((), (), s32[]{:S(2)}) async-start(), calls=%async_computation.7 | async-start | bytes 3244032 | tf_op jit(solution)/shard_map/all_gather | solution.py:93
  7.9 75.8 %all-gather.23.cloned.1.call-start = ((), (), s32[]{:S(2)}) async-start(), calls=%async_computation.9 | async-start | bytes 3244032 | tf_op jit(solution)/shard_map/all_gather | solution.py:98
  8.7 111.9 %all-gather.13.cloned.1.call-start = ((), (), s32[]{:S(2)}) async-start(), calls=%async_computation.4 | async-start | bytes 3244032 | tf_op jit(solution)/shard_map/all_gather | solution.py:91
  9.4 147.8 %all-gather.21.cloned.1.call-start = ((), (), s32[]{:S(2)}) async-start(), calls=%async_computation.8 | async-start | bytes 3244032 | tf_op jit(solution)/shard_map/all_gather | solution.py:94
  10.0 184.0 %all-gather.15.cloned.1.call-start = ((), (), s32[]{:S(2)}) async-start(), calls=%async_computation.5 | async-start | bytes 3244032 | tf_op jit(solution)/shard_map/all_gather | solution.py:92
  10.6 220.1 %all-gather.17.cloned.1.call-start = ((), (), s32[]{:S(2)}) async-start(), calls=%async_computation.6 | async-start | bytes 3244032 | tf_op jit(solution)/shard_map/all_gather | solution.py:97
  11.2 72.5 %copy-start.15 = (bf16[128,2048]{1,0:T(8,128)(2,1)S(1)}, bf16[128,2048]{1,0:T(8,128)(2,1)}, u32[]{:S(2)}) copy-start(bf16[128,2048]{1,0:T(8,128)(2,1)} %param.21) | copy-start | bytes 1572868
  11.2 277.2 %all-reduce.7.cloned.1.call-start = ((), (), s32[]{:S(2)}) async-start(), calls=%async_computation.17 | async-start | bytes 2097152 | tf_op jit(solution)/shard_map/psum | solution.py:22
  12.9 74.2 %copy-start.10 = (bf16[128,2048]{1,0:T(8,128)(2,1)}, bf16[128,2048]{1,0:T(8,128)(2,1)S(1)}, u32[]{:S(2)}) copy-start(bf16[128,2048]{1,0:T(8,128)(2,1)S(1)} %fusion.12) | copy-start | bytes 1572868
  12.9 107.6 %copy-start.23 = (f32[2048]{0:T(1024)S(1)}, f32[2048]{0:T(1024)}, u32[]{:S(2)}) copy-start(f32[2048]{0:T(1024)} %param.22) | copy-start | bytes 24580
  124.1 37.0 %copy-start = (bf16[2048,704]{0,1:T(8,128)(2,1)S(1)}, bf16[2048,704]{0,1:T(8,128)(2,1)}, u32[]{:S(2)}) copy-start(bf16[2048,704]{0,1:T(8,128)(2,1)} %all-gather.19.cloned.1.call-done) | copy-start | bytes 8650756
  236.7 125.9 %all-reduce.5.cloned.1.call-start = ((), (), s32[]{:S(2)}) async-start(), calls=%async_computation.16 | async-start | bytes 2097152 | tf_op jit(solution)/shard_map/psum | solution.py:22
  293.3 78.7 %copy-start.4 = (bf16[128,2048]{1,0:T(8,128)(2,1)}, bf16[128,2048]{1,0:T(8,128)(2,1)S(1)}, u32[]{:S(2)}) copy-start(bf16[128,2048]{1,0:T(8,128)(2,1)S(1)} %get-tuple-element.14) | copy-start | bytes 1572868
  310.0 11.2 %copy-start.11 = (bf16[128,2048]{1,0:T(8,128)(2,1)S(1)}, bf16[128,2048]{1,0:T(8,128)(2,1)}, u32[]{:S(2)}) copy-start(bf16[128,2048]{1,0:T(8,128)(2,1)} %copy-done.10) | copy-start | bytes 1572868
  310.0 29.9 %copy-start.14 = (bf16[128,2048]{1,0:T(8,128)(2,1)S(1)}, bf16[128,2048]{1,0:T(8,128)(2,1)}, u32[]{:S(2)}) copy-start(bf16[128,2048]{1,0:T(8,128)(2,1)} %copy-done.12) | copy-start | bytes 1572868
  310.0 91.6 %all-gather.33.cloned.1.call-start = ((), (), s32[]{:S(2)}) async-start(), calls=%async_computation.14 | async-start | bytes 1622016 | tf_op jit(solution)/shard_map/all_gather | solution.py:114
  310.8 118.9 %all-gather.31.cloned.1.call-start = ((), (), s32[]{:S(2)}) async-start(), calls=%async_computation.13 | async-start | bytes 1622016 | tf_op jit(solution)/shard_map/all_gather | solution.py:113
  311.4 154.2 %all-gather.35.cloned.1.call-start = ((), (), s32[]{:S(2)}) async-start(), calls=%async_computation.15 | async-start | bytes 1622016 | tf_op jit(solution)/shard_map/all_gather | solution.py:115
  312.1 179.9 %all-gather.27.cloned.1.call-start = ((), (), s32[]{:S(2)}) async-start(), calls=%async_computation.11 | async-start | bytes 1622016 | tf_op jit(solution)/shard_map/all_gather | solution.py:114
  312.7 206.0 %all-gather.25.cloned.1.call-start = ((), (), s32[]{:S(2)}) async-start(), calls=%async_computation.10 | async-start | bytes 1622016 | tf_op jit(solution)/shard_map/all_gather | solution.py:113
  315.5 25.5 %copy-start.9 = (bf16[128,2048]{1,0:T(8,128)(2,1)S(1)}, bf16[128,2048]{1,0:T(8,128)(2,1)}, u32[]{:S(2)}) copy-start(bf16[128,2048]{1,0:T(8,128)(2,1)} %copy-done.8) | copy-start | bytes 1572868
  315.5 17.6 %all-to-all-start.3 = ((bf16[128,8,256]{0,2,1:T(8,128)(2,1)}), bf16[128,8,256]{0,2,1:T(8,128)(2,1)S(1)}, u32[]{:S(2)}, u32[]{:S(2)}) async-start(bf16[128,8,256]{0,2,1:T(8,128)(2,1)} %bitcast.8), calls=%async_computation.3 | async-start | bytes 1048576 | tf_op jit(solution)/shard_map/all_to_all | solution.py:109
  321.2 41.5 %copy-start.7 = (bf16[128,2048]{1,0:T(8,128)(2,1)S(1)}, bf16[128,2048]{1,0:T(8,128)(2,1)}, u32[]{:S(2)}) copy-start(bf16[128,2048]{1,0:T(8,128)(2,1)} %param.19) | copy-start | bytes 1572868
  333.0 33.3 %all-to-all-start.2 = ((bf16[128,8,256]{2,0,1:T(8,128)(2,1)}), bf16[128,8,256]{2,0,1:T(8,128)(2,1)S(1)}, u32[]{:S(2)}, u32[]{:S(2)}) async-start(bf16[128,8,256]{2,0,1:T(8,128)(2,1)} %bitcast.59), calls=%async_computation.2 | async-start | bytes 1048576 | tf_op jit(solution)/shard_map/all_to_all | solution.py:108
  339.9 205.2 %all-gather.29.cloned.1.call-start = ((), (), s32[]{:S(2)}) async-start(), calls=%async_computation.12 | async-start | bytes 1622016 | tf_op jit(solution)/shard_map/all_gather | solution.py:115
  362.6 39.0 %copy-start.16 = (f32[256,704]{0,1:T(8,128)S(1)}, f32[256,704]{0,1:T(8,128)}, u32[]{:S(2)}) copy-start(f32[256,704]{0,1:T(8,128)} %param.34) | copy-start | bytes 2162692
  366.3 66.2 %all-to-all-start = ((bf16[128,8,256]{2,0,1:T(8,128)(2,1)}), bf16[128,8,256]{2,0,1:T(8,128)(2,1)S(1)}, u32[]{:S(2)}, u32[]{:S(2)}) async-start(bf16[128,8,256]{2,0,1:T(8,128)(2,1)} %bitcast.61), calls=%async_computation | async-start | bytes 1048576 | tf_op jit(solution)/shard_map/all_to_all | solution.py:108
  404.4 61.1 %copy-start.17 = (f32[704,256]{1,0:T(8,128)S(1)}, f32[704,256]{1,0:T(8,128)}, u32[]{:S(2)}) copy-start(f32[704,256]{1,0:T(8,128)} %param.35) | copy-start | bytes 2162692
  432.6 59.4 %copy-start.18 = (f32[256,704]{0,1:T(8,128)S(1)}, f32[256,704]{0,1:T(8,128)}, u32[]{:S(2)}) copy-start(f32[256,704]{0,1:T(8,128)} %param.31) | copy-start | bytes 2162692
  432.6 88.8 %all-to-all-start.1 = ((bf16[128,8,256]{2,0,1:T(8,128)(2,1)}), bf16[128,8,256]{2,0,1:T(8,128)(2,1)S(1)}, u32[]{:S(2)}, u32[]{:S(2)}) async-start(bf16[128,8,256]{2,0,1:T(8,128)(2,1)} %bitcast.60), calls=%async_computation.1 | async-start | bytes 1048576 | tf_op jit(solution)/shard_map/all_to_all | solution.py:109
  468.3 50.4 %copy-start.19 = (f32[256,704]{0,1:T(8,128)S(1)}, f32[256,704]{0,1:T(8,128)}, u32[]{:S(2)}) copy-start(f32[256,704]{0,1:T(8,128)} %param.30) | copy-start | bytes 2162692
  492.0 53.1 %copy-start.20 = (f32[704,256]{1,0:T(8,128)S(1)}, f32[704,256]{1,0:T(8,128)}, u32[]{:S(2)}) copy-start(f32[704,256]{1,0:T(8,128)} %param.32) | copy-start | bytes 2162692
  (10 other events, 38.1 us)
Sparse Core Ops, SparseCore 0:
  9.6 37.1 all-gather.18
  48.4 35.2 all-gather.22
  85.3 35.2 all-gather.12
  122.0 35.2 all-gather.20
  158.7 35.2 all-gather.14
  195.4 35.2 all-gather.16
  236.8 51.4 all-reduce.6
  310.2 52.4 all-reduce.4
  364.2 37.4 all-gather.32
  403.7 25.9 all-gather.30
  431.8 33.6 all-gather.34
  467.0 24.9 all-gather.26
  493.6 24.9 all-gather.24
  520.1 24.9 all-gather.28
where the time goes:
time: 556 us; the launch traced here: 554 us
  waiting for transfers between devices  434 us (78%)
  matrix products  63.4 us (11%)
  starting transfers between devices  22.5 us (4%)
  other arithmetic  14.7 us (3%)
  between operations  14.2 us (3%)
  local copies, waits for them, and re-layouts  5.63 us (1%)
    psum x2, waiting for transfers between devices, block_forward(): lax.psum(jnp.dot(hidden, w_down, preferred_element_type=jnp.float32).asty...  65.5 us
    all_gather x2, waiting for transfers between devices, collect(): lax.all_gather(hidden, 'fs', axis=0, tiled=True)  53.1 us
    all_gather x2, waiting for transfers between devices, collect(): lax.all_gather(up_grad, 'fs', axis=0, tiled=True)  51.4 us
    all_gather x2, waiting for transfers between devices, collect(): lax.all_gather(gate_grad, 'fs', axis=0, tiled=True)  49 us
    all_gather x1, waiting for transfers between devices, per_device(): lax.all_gather(down_first, 'fs', axis=1, tiled=True)  36.7 us
    all_gather x1, waiting for transfers between devices, per_device(): lax.all_gather(gate_second, 'fs', axis=0, tiled=True)  33.9 us
    all_gather x1, waiting for transfers between devices, per_device(): lax.all_gather(gate_first, 'fs', axis=0, tiled=True)  33.4 us
    all_gather x1, waiting for transfers between devices, per_device(): lax.all_gather(down_second, 'fs', axis=1, tiled=True)  33.4 us
  transfers between devices with their start and end apart: 18, of which 15 were waited for; matrix products, arithmetic and copies ran while one was open for 9% of the time, Pallas kernels for 0%

commit v1 on v0

v1 whole, which is shorter than its diff:
```python
import jax
import jax.numpy as jnp
from jax import lax
from jax.sharding import PartitionSpec as P

norm_eps = 1e-06


def normalize(values, gain_vector):
    widened = values.astype(jnp.float32)
    factor = lax.rsqrt(jnp.mean(widened * widened, axis=-1, keepdims=True) + norm_eps)
    normed = (widened * factor * gain_vector).astype(jnp.bfloat16)
    return (widened, factor, normed)


def project(rows, weights):
    return jnp.dot(rows, weights, preferred_element_type=jnp.float32)


def project_back(hidden_rows, weights):
    return jnp.einsum("tf,df->td", hidden_rows, weights, preferred_element_type=jnp.float32)


def fold_rows(left, right):
    return jnp.einsum("ta,tb->ab", left, right, preferred_element_type=jnp.float32)


def own_rows(rows):
    count = rows.shape[0] // lax.axis_size("tp")
    return lax.dynamic_slice_in_dim(rows, lax.axis_index("tp") * count, count, axis=0)


def sum_rows(partial):
    shares = lax.all_to_all(
        partial.astype(jnp.bfloat16), "tp", split_axis=0, concat_axis=0, tiled=True
    )
    shares = shares.reshape((lax.axis_size("tp"), -1, shares.shape[1]))
    return jnp.sum(shares.astype(jnp.float32), axis=0)


def join_rows(rows):
    return lax.all_gather(rows, "tp", axis=0, tiled=True)


def block_forward(values, gain_vector, weights, width):
    widened, factor, normed = normalize(values, gain_vector)
    pre = project(normed, weights[:, : 2 * width])
    hidden = (jax.nn.silu(pre[:, :width]) * pre[:, width:]).astype(jnp.bfloat16)
    branch = sum_rows(project_back(hidden, weights[:, 2 * width :]))
    return join_rows((own_rows(widened) + 0.5 * branch).astype(jnp.bfloat16))


def block_backward(normalized, cotangent, weights, width):
    widened, factor, normed = normalized
    pre = project(normed, weights[:, : 2 * width])
    gate_pre, up_pre = pre[:, :width], pre[:, width:]
    sigmoid_gate = jax.nn.sigmoid(gate_pre)
    activated = gate_pre * sigmoid_gate
    hidden = (activated * up_pre).astype(jnp.bfloat16)
    hidden_grad = 0.5 * project(cotangent, weights[:, 2 * width :])
    gate_grad = (
        hidden_grad * up_pre * sigmoid_gate * (1.0 + gate_pre * (1.0 - sigmoid_gate))
    ).astype(jnp.bfloat16)
    up_grad = (hidden_grad * activated).astype(jnp.bfloat16)
    pieces = jnp.concatenate((gate_grad, up_grad, hidden), axis=1)
    partial_value = project_back(pieces[:, : 2 * width], weights[:, : 2 * width])
    return (partial_value, pieces)


def backward_rows(normalized, cotangent, gain_vector, partial_value):
    normed_grad = sum_rows(partial_value)
    widened, factor = own_rows(normalized[0]), own_rows(normalized[1])
    scaled = normed_grad * gain_vector
    unit_rows = widened * factor
    rows_grad = own_rows(cotangent).astype(jnp.float32) + factor * (
        scaled - unit_rows * jnp.mean(scaled * unit_rows, axis=-1, keepdims=True)
    )
    return rows_grad.astype(jnp.bfloat16)


def gather_weights(gate, up, down):
    return lax.all_gather(jnp.concatenate((gate, up, down.T), axis=1), "fs", axis=0, tiled=True)


def share_columns(rows):
    return lax.all_to_all(rows, "fs", split_axis=1, concat_axis=0, tiled=True)


def join_columns(share):
    joined = join_rows(share)
    parts = joined.reshape((lax.axis_size("tp"), lax.axis_size("fs"), -1, joined.shape[1]))
    return jnp.swapaxes(parts, 0, 1).reshape(joined.shape)


def per_device(
    late_input,
    early_input,
    early_mid,
    cotangent,
    gain_first,
    gain_second,
    gate_first,
    up_first,
    down_first,
    gate_second,
    up_second,
    down_second,
    sum_gate_first,
    sum_up_first,
    sum_down_first,
    sum_gate_second,
    sum_up_second,
    sum_down_second,
):
    width = gate_first.shape[1]
    weights_second = gather_weights(gate_second, up_second, down_second)
    weights_first = gather_weights(gate_first, up_first, down_first)
    norm_second = normalize(early_mid, gain_second)
    norm_first = normalize(early_input, gain_first)
    early_rows = jnp.stack(
        (own_rows(norm_second[2]), own_rows(norm_first[2]), own_rows(cotangent))
    )
    early_shares = lax.all_to_all(early_rows, "fs", split_axis=2, concat_axis=1, tiled=True)
    columns_second = join_columns(early_shares[0])
    columns_first = join_columns(early_shares[1])
    columns_cotangent = join_columns(early_shares[2])
    weights_second, columns_second, columns_first, columns_cotangent = lax.optimization_barrier(
        (weights_second, columns_second, columns_first, columns_cotangent)
    )

    partial_second, pieces_second = block_backward(
        norm_second, cotangent, weights_second, width
    )
    all_second = lax.all_gather(pieces_second, "fs", axis=0, tiled=True)
    mid_rows = backward_rows(norm_second, cotangent, gain_second, partial_second)
    mid_grad = join_rows(mid_rows)
    columns_mid = join_columns(share_columns(mid_rows))
    weights_first, pieces_second, mid_grad, columns_mid = lax.optimization_barrier(
        (weights_first, pieces_second, mid_grad, columns_mid)
    )
    partial_first, pieces_first = block_backward(norm_first, mid_grad, weights_first, width)
    all_first = lax.all_gather(pieces_first, "fs", axis=0, tiled=True)
    late_mid = block_forward(late_input, gain_first, weights_first, width)
    input_grad = join_rows(backward_rows(norm_first, mid_grad, gain_first, partial_first))
    late_out = block_forward(late_mid, gain_second, weights_second, width)
    all_second, late_out, input_grad = lax.optimization_barrier((all_second, late_out, input_grad))

    def collect(pieces, columns_in, columns_out, sums):
        return (
            sums[0] + fold_rows(columns_in, pieces[:, :width]),
            sums[1] + fold_rows(columns_in, pieces[:, width : 2 * width]),
            sums[2] + 0.5 * fold_rows(pieces[:, 2 * width :], columns_out),
        )

    new_second = collect(
        all_second, columns_second, columns_cotangent, (sum_gate_second, sum_up_second, sum_down_second)
    )
    all_first, new_second = lax.optimization_barrier((all_first, new_second))
    new_first = collect(
        all_first, columns_first, columns_mid, (sum_gate_first, sum_up_first, sum_down_first)
    )
    return (late_mid, late_out, input_grad) + new_first + new_second


def solution(mesh):
    in_specs = (
        P("fs", None),
        P("fs", None),
        P("fs", None),
        P("fs", None),
        P(),
        P(),
        P("fs", "tp"),
        P("fs", "tp"),
        P("tp", "fs"),
        P("fs", "tp"),
        P("fs", "tp"),
        P("tp", "fs"),
        P("fs", "tp"),
        P("fs", "tp"),
        P("tp", "fs"),
        P("fs", "tp"),
        P("fs", "tp"),
        P("tp", "fs"),
    )
    out_specs = (
        P("fs", None),
        P("fs", None),
        P("fs", None),
        P("fs", "tp"),
        P("fs", "tp"),
        P("tp", "fs"),
        P("fs", "tp"),
        P("fs", "tp"),
        P("tp", "fs"),
    )
    return jax.shard_map(
        per_device, mesh=mesh, in_specs=in_specs, out_specs=out_specs, check_vma=False
    )
```

time: 556 us -> 317 us (0.57)
  waiting for transfers between devices: 434 us -> 85.3 us
  blocking collectives: 0 us -> 105 us
  local copies, waits for them, and re-layouts: 5.63 us -> 13.9 us
  matrix products: 63.4 us -> 56.7 us
    all_gather x12 -> x4, waiting for transfers between devices: 351 us -> 67.6 us  [the longest x2 60.8 us: gather_weights(): lax.all_gather(jnp.concatenate((gate, up, down.T), axis=1), 'fs', axis=0,...]
    all_gather x0 -> x8, blocking collectives: none -> 75.1 us  [join_rows(): return lax.all_gather(rows, 'tp', axis=0, tiled=True)]
    psum x2 -> x0, waiting for transfers between devices: 65.5 us -> none  [block_forward(): lax.psum(jnp.dot(hidden, w_down, preferred_element_type=jnp.float32).asty...]
    all_to_all x0 -> x1, blocking collectives: none -> 29.6 us  [per_device(): lax.all_to_all(early_rows, 'fs', split_axis=2, concat_axis=1, tiled=True)]
    dot_general x20 -> x16, matrix products: 63.4 us -> 56.7 us  [the longest x6 23.6 us: project(): return jnp.dot(rows, weights, preferred_element_type=jnp.float32)]
    unnamed x14 -> x4, waiting for transfers between devices: 6.8 us -> 0.07 us
    all_to_all x4 -> x5, waiting for transfers between devices: 11 us -> 17.6 us  [the longest x4 9.9 us: sum_rows(): lax.all_to_all(partial.astype(jnp.bfloat16), 'tp', split_axis=0, concat_a...]
    all_to_all x4 -> x5, starting transfers between devices: 21.8 us -> 20 us  [the longest x4 14.6 us: sum_rows(): lax.all_to_all(partial.astype(jnp.bfloat16), 'tp', split_axis=0, concat_a...]
  transfers between devices with their start and end apart: 18 -> 9, of which waited for: 15 -> 6; matrix products, arithmetic and copies ran while one was open for 9% -> 23% of each run, Pallas kernels for 0% -> 0%
where the time goes in v1:
time: 317 us; the launch traced here: 312 us
  blocking collectives  105 us (33%)
  waiting for transfers between devices  85.3 us (27%)
  matrix products  56.7 us (18%)
  starting transfers between devices  20.1 us (6%)
  other arithmetic  16.7 us (5%)
  between operations  14.2 us (4%)
  local copies, waits for them, and re-layouts  13.9 us (4%)
    all_gather x8, blocking collectives, join_rows(): return lax.all_gather(rows, 'tp', axis=0, tiled=True)  75.1 us
    all_gather x2, waiting for transfers between devices, gather_weights(): lax.all_gather(jnp.concatenate((gate, up, down.T), axis=1), 'fs', axis=0,...  60.8 us
    all_to_all x1, blocking collectives, per_device(): lax.all_to_all(early_rows, 'fs', split_axis=2, concat_axis=1, tiled=True)  29.6 us
    dot_general x6, matrix products, project(): return jnp.dot(rows, weights, preferred_element_type=jnp.float32)  23.6 us
    dot_general x6, matrix products, fold_rows(): jnp.einsum('ta,tb->ab', left, right, preferred_element_type=jnp.float32)  17 us
    dot_general x4, matrix products, project_back(): jnp.einsum('tf,df->td', hidden_rows, weights, preferred_element_type=jnp....  16 us
    all_to_all x4, starting transfers between devices, sum_rows(): lax.all_to_all(partial.astype(jnp.bfloat16), 'tp', split_axis=0, concat_a...  14.6 us
    all_to_all x4, waiting for transfers between devices, sum_rows(): lax.all_to_all(partial.astype(jnp.bfloat16), 'tp', split_axis=0, concat_a...  9.9 us
  transfers between devices with their start and end apart: 9, of which 6 were waited for; matrix products, arithmetic and copies ran while one was open for 23% of the time, Pallas kernels for 0%

profile of v1, /device:TPU:9, one launch (start us, length us, event | category | flops | bytes accessed | tf_op | source)
XLA Modules:
  0.0 311.7 jit_solution(12072726947669320214)
XLA Ops:
  16.5 29.6 %all_to_all.70 = bf16[8,2,12288]{2,1,0:T(2,128)(2,1)} all-to-all(bf16[8,2,12288]{2,1,0:T(2,128)(2,1)S(1)} %reshape.147), channel_id=1, replica_groups=mesh['fs'=8,'tp'=4] {'fs'}, dimensions={0} | all-to-all | bytes 786432 | tf_op jit(solution)/shard_map/all_to_all | solution.py:123
  50.1 8.9 %all_gather.38 = bf16[1024,256]{1,0:T(8,128)(2,1)S(1)} all-gather(bf16[256,256]{1,0:T(8,128)(2,1)S(1)} %bitcast.67), channel_id=1, replica_groups=mesh['fs'=8,'tp'=4] {'tp'}, dimensions={0}, use_global_device_ids=true | all-gather | bytes 655360 | tf_op jit(solution)/shard_map/all_gather | solution.py:42
  59.1 8.6 %all_gather.39 = bf16[1024,256]{1,0:T(8,128)(2,1)S(1)} all-gather(bf16[256,256]{1,0:T(8,128)(2,1)S(1)} %bitcast.68), channel_id=1, replica_groups=mesh['fs'=8,'tp'=4] {'tp'}, dimensions={0}, use_global_device_ids=true | all-gather | bytes 655360 | tf_op jit(solution)/shard_map/all_gather | solution.py:42
  67.8 8.4 %all_gather.40 = bf16[1024,256]{1,0:T(8,128)(2,1)S(1)} all-gather(bf16[256,256]{1,0:T(8,128)(2,1)S(1)} %bitcast.69), channel_id=1, replica_groups=mesh['fs'=8,'tp'=4] {'tp'}, dimensions={0}, use_global_device_ids=true | all-gather | bytes 655360 | tf_op jit(solution)/shard_map/all_gather | solution.py:42
  77.0 28.6 %all-gather.7.cloned.1.call-done = bf16[2048,2112]{0,1:T(8,128)(2,1)} async-done(((bf16[256,2112]{0,1:T(8,128)(2,1)}), bf16[2048,2112]{0,1:T(8,128)(2,1)}) %all-gather.7.cloned.1.call-update) | async-done | bytes 8650768 | tf_op jit(solution)/shard_map/all_gather | solution.py:82
  105.6 4.4 %fusion.10 = f32[128,1408]{0,1:T(8,128)S(1)} fusion(bf16[128,2048]{1,0:T(8,128)(2,1)S(1)} %copy-done.6, bf16[2048,2112]{0,1:T(8,128)(2,1)} %all-gather.7.cloned.1.call-done), kind=kOutput, calls=%fused_computation.10 | convolution fusion | flops 738197504 | bytes 7012352 | tf_op jit(solution)/shard_map/dot_general | solution.py:17
  113.6 5.0 %fusion.26 = bf16[128,2048]{1,0:T(8,128)(2,1)} fusion(bf16[2048,2112]{0,1:T(8,128)(2,1)} %all-gather.7.cloned.1.call-done, bf16[128,704]{0,1:T(8,128)(2,1)S(1)} %get-tuple-element.40, bf16[128,704]{0,1:T(8,128)(2,1)S(1)} %get-tuple-element.39), kind=kOutput, calls=%fused_computation.22 | convolution fusion | flops 739180544 | bytes 6651904 | tf_op jit(solution)/shard_map/tf,df->td/dot_general | solution.py:21
  118.7 3.5 %all-to-all-start.1 = ((bf16[4,32,2048]{2,1,0:T(8,128)(2,1)}), bf16[4,32,2048]{2,1,0:T(8,128)(2,1)S(1)}, u32[]{:S(2)}, u32[]{:S(2)}) async-start(bf16[4,32,2048]{2,1,0:T(8,128)(2,1)} %bitcast.20), calls=%async_computation.1 | async-start | bytes 1048576 | tf_op jit(solution)/shard_map/all_to_all | solution.py:34
  123.3 6.5 %all-to-all-done.1 = bf16[4,32,2048]{2,1,0:T(8,128)(2,1)S(1)} async-done(((bf16[4,32,2048]{2,1,0:T(8,128)(2,1)}), bf16[4,32,2048]{2,1,0:T(8,128)(2,1)S(1)}, u32[]{:S(2)}, u32[]{:S(2)}) %all-to-all-start.1) | async-done | bytes 524320 | tf_op jit(solution)/shard_map/all_to_all | solution.py:34
  133.0 5.4 %all-to-all-start.2 = ((bf16[32,8,256]{2,0,1:T(8,128)(2,1)}), bf16[32,8,256]{2,0,1:T(8,128)(2,1)S(1)}, u32[]{:S(2)}, u32[]{:S(2)}) async-start(bf16[32,8,256]{2,0,1:T(8,128)(2,1)} %bitcast.53), calls=%async_computation.2 | async-start | bytes 262144 | tf_op jit(solution)/shard_map/all_to_all | solution.py:86
  138.4 8.7 %all_gather.41 = bf16[128,2048]{1,0:T(8,128)(2,1)S(1)} all-gather(bf16[32,2048]{1,0:T(8,128)(2,1)S(1)} %add_convert_fusion.3), channel_id=1, replica_groups=mesh['fs'=8,'tp'=4] {'tp'}, dimensions={0}, use_global_device_ids=true | all-gather | bytes 655360 | tf_op jit(solution)/shard_map/all_gather | solution.py:42
  147.1 7.7 %all-to-all-done.2 = bf16[32,8,256]{2,0,1:T(8,128)(2,1)S(1)} async-done(((bf16[32,8,256]{2,0,1:T(8,128)(2,1)}), bf16[32,8,256]{2,0,1:T(8,128)(2,1)S(1)}, u32[]{:S(2)}, u32[]{:S(2)}) %all-to-all-start.2) | async-done | bytes 131104 | tf_op jit(solution)/shard_map/all_to_all | solution.py:86
  154.8 8.7 %all_gather.42 = bf16[1024,256]{1,0:T(8,128)(2,1)S(1)} all-gather(bf16[256,256]{1,0:T(8,128)(2,1)S(1)} %bitcast.66), channel_id=1, replica_groups=mesh['fs'=8,'tp'=4] {'tp'}, dimensions={0}, use_global_device_ids=true | all-gather | bytes 655360 | tf_op jit(solution)/shard_map/all_gather | solution.py:42
  164.3 32.2 %all-gather.5.cloned.1.call-done = bf16[2048,2112]{0,1:T(8,128)(2,1)} async-done(((bf16[256,2112]{0,1:T(8,128)(2,1)}), bf16[2048,2112]{0,1:T(8,128)(2,1)}) %all-gather.5.cloned.1.call-update) | async-done | bytes 8650768 | tf_op jit(solution)/shard_map/all_gather | solution.py:82
  196.5 4.5 %fusion.2 = f32[128,1408]{0,1:T(8,128)S(1)} fusion(bf16[128,2048]{1,0:T(8,128)(2,1)} %copy-done.4, bf16[2048,2112]{0,1:T(8,128)(2,1)} %all-gather.5.cloned.1.call-done), kind=kOutput, calls=%fused_computation.2 | convolution fusion | flops 738197504 | bytes 7012352 | tf_op jit(solution)/shard_map/dot_general | solution.py:17
  206.3 4.8 %fusion.4 = f32[128,1408]{0,1:T(8,128)S(1)} fusion(bf16[2048,2112]{0,1:T(8,128)(2,1)} %all-gather.5.cloned.1.call-done, f32[2048]{0:T(1024)S(1)} %copy-done.17, f32[128]{0:T(128)S(1)} %add_rsqrt_fusion.3, bf16[128,2048]{1,0:T(8,128)(2,1)S(1)} %copy-done.2), kind=kOutput, calls=%fused_computation.4 | convolution fusion | flops 739246080 | bytes 7021056 | tf_op jit(solution)/shard_map/dot_general | solution.py:17
  211.0 3.3 %fusion.23 = bf16[128,2048]{1,0:T(8,128)(2,1)} fusion(bf16[2048,2112]{0,1:T(8,128)(2,1)} %all-gather.5.cloned.1.call-done, f32[128,1408]{0,1:T(8,128)S(1)} %fusion.4), kind=kOutput, calls=%fused_computation.21 | convolution fusion | flops 369901568 | bytes 4128768 | tf_op jit(solution)/shard_map/tf,df->td/dot_general | solution.py:21
  214.3 3.5 %all-to-all-start.3 = ((bf16[4,32,2048]{2,1,0:T(8,128)(2,1)}), bf16[4,32,2048]{2,1,0:T(8,128)(2,1)S(1)}, u32[]{:S(2)}, u32[]{:S(2)}) async-start(bf16[4,32,2048]{2,1,0:T(8,128)(2,1)} %bitcast.26), calls=%async_computation.3 | async-start | bytes 1048576 | tf_op jit(solution)/shard_map/all_to_all | solution.py:34
  217.8 4.5 %fusion.29 = bf16[128,2048]{1,0:T(8,128)(2,1)} fusion(bf16[2048,2112]{0,1:T(8,128)(2,1)} %all-gather.5.cloned.1.call-done, bf16[128,704]{0,1:T(8,128)(2,1)S(1)} %get-tuple-element.38, bf16[128,704]{0,1:T(8,128)(2,1)S(1)} %get-tuple-element.37), kind=kOutput, calls=%fused_computation.23 | convolution fusion | flops 739180544 | bytes 6651904 | tf_op jit(solution)/shard_map/tf,df->td/dot_general | solution.py:21
  222.3 3.4 %all-to-all-done.3 = bf16[4,32,2048]{2,1,0:T(8,128)(2,1)S(1)} async-done(((bf16[4,32,2048]{2,1,0:T(8,128)(2,1)}), bf16[4,32,2048]{2,1,0:T(8,128)(2,1)S(1)}, u32[]{:S(2)}, u32[]{:S(2)}) %all-to-all-start.3) | async-done | bytes 524320 | tf_op jit(solution)/shard_map/all_to_all | solution.py:34
  225.6 3.5 %all-to-all-start.5 = ((bf16[4,32,2048]{2,1,0:T(8,128)(2,1)}), bf16[4,32,2048]{2,1,0:T(8,128)(2,1)S(1)}, u32[]{:S(2)}, u32[]{:S(2)}) async-start(bf16[4,32,2048]{2,1,0:T(8,128)(2,1)} %bitcast.72), calls=%async_computation.5 | async-start | bytes 1048576 | tf_op jit(solution)/shard_map/all_to_all | solution.py:34
  230.2 11.4 %all_gather.43 = bf16[128,2048]{1,0:T(8,128)(2,1)S(1)} all-gather(bf16[32,2048]{1,0:T(8,128)(2,1)S(1)} %add_convert_fusion.2), channel_id=1, replica_groups=mesh['fs'=8,'tp'=4] {'tp'}, dimensions={0}, use_global_device_ids=true | all-gather | bytes 655360 | tf_op jit(solution)/shard_map/all_gather | solution.py:42
  241.8 4.5 %fusion.6 = f32[128,1408]{0,1:T(8,128)S(1)} fusion(bf16[2048,2112]{0,1:T(8,128)(2,1)} %all-gather.7.cloned.1.call-done, f32[128]{0:T(128)S(1)} %add_rsqrt_fusion, bf16[128,2048]{1,0:T(8,128)(2,1)S(1)} %all_gather.43, f32[2048]{0:T(1024)S(1)} %copy-done.16), kind=kOutput, calls=%fused_computation.6 | convolution fusion | flops 739246080 | bytes 7021056 | tf_op jit(solution)/shard_map/dot_general | solution.py:17
  247.4 3.3 %fusion.20 = bf16[128,2048]{1,0:T(8,128)(2,1)} fusion(bf16[2048,2112]{0,1:T(8,128)(2,1)} %all-gather.7.cloned.1.call-done, f32[128,1408]{0,1:T(8,128)S(1)} %fusion.6), kind=kOutput, calls=%fused_computation.20 | convolution fusion | flops 369901568 | bytes 4128768 | tf_op jit(solution)/shard_map/tf,df->td/dot_general | solution.py:21
  250.7 4.1 %all-to-all-start.4 = ((bf16[4,32,2048]{2,1,0:T(8,128)(2,1)}), bf16[4,32,2048]{2,1,0:T(8,128)(2,1)}, u32[]{:S(2)}, u32[]{:S(2)}) async-start(bf16[4,32,2048]{2,1,0:T(8,128)(2,1)} %bitcast.73), calls=%async_computation.4 | async-start | bytes 1048576 | tf_op jit(solution)/shard_map/all_to_all | solution.py:34
  256.2 10.7 %all_gather.46 = bf16[128,2048]{1,0:T(8,128)(2,1)S(1)} all-gather(bf16[32,2048]{1,0:T(8,128)(2,1)S(1)} %add_convert_fusion), channel_id=1, replica_groups=mesh['fs'=8,'tp'=4] {'tp'}, dimensions={0}, use_global_device_ids=true | all-gather | bytes 655360 | tf_op jit(solution)/shard_map/all_gather | solution.py:42
  269.1 9.7 %all_gather.45 = bf16[128,2048]{1,0:T(8,128)(2,1)S(1)} all-gather(bf16[32,2048]{1,0:T(8,128)(2,1)S(1)} %add_convert_fusion.1), channel_id=1, replica_groups=mesh['fs'=8,'tp'=4] {'tp'}, dimensions={0}, use_global_device_ids=true | all-gather | bytes 655360 | tf_op jit(solution)/shard_map/all_gather | solution.py:42
  278.9 2.9 fusion.47
  281.8 2.8 fusion.44
  287.4 6.9 %all-gather.11.cloned.1.call-done = bf16[1024,2112]{0,1:T(8,128)(2,1)} async-done(((bf16[128,2112]{0,1:T(8,128)(2,1)}), bf16[1024,2112]{0,1:T(8,128)(2,1)}) %all-gather.11.cloned.1.call-update) | async-done | bytes 4325392 | tf_op jit(solution)/shard_map/all_gather | solution.py:142
  294.2 2.8 fusion.59
  297.1 2.9 fusion.56
  (114 shorter events, 41.8 us)
Async XLA Ops:
  7.2 2.6 copy-start.12
  7.2 2.6 copy-start.14
  7.2 2.6 copy-start.13
  7.2 98.4 %all-gather.7.cloned.1.call-start = ((), (), s32[]{:S(2)}) async-start(), calls=%async_computation.7 | async-start | bytes 9732096 | tf_op jit(solution)/shard_map/all_gather | solution.py:82
  7.3 3.7 %copy-start.1 = (bf16[128,2048]{1,0:T(8,128)(2,1)S(1)}, bf16[128,2048]{1,0:T(8,128)(2,1)}, u32[]{:S(2)}) copy-start(bf16[128,2048]{1,0:T(8,128)(2,1)} %param.19) | copy-start | bytes 1572868
  9.6 1.5 copy-start
  9.6 2.6 copy-start.17
  9.7 2.8 copy-start.16
  9.7 186.8 %all-gather.5.cloned.1.call-start = ((), (), s32[]{:S(2)}) async-start(), calls=%async_computation.6 | async-start | bytes 9732096 | tf_op jit(solution)/shard_map/all_gather | solution.py:82
  10.9 267.9 %all-gather.9.cloned.1.call-start = ((), (), s32[]{:S(2)}) async-start(), calls=%async_computation.8 | async-start | bytes 4866048 | tf_op jit(solution)/shard_map/all_gather | solution.py:134
  11.3 1.4 copy-start.18
  11.3 1.4 copy-start.20
  12.5 0.8 copy-start.4
  50.1 55.5 %copy-start.6 = (bf16[128,2048]{1,0:T(8,128)(2,1)S(1)}, bf16[128,2048]{1,0:T(8,128)(2,1)}, u32[]{:S(2)}) copy-start(bf16[128,2048]{1,0:T(8,128)(2,1)} %copy-done.5) | copy-start | bytes 1572868
  105.6 4.4 %copy-start.15 = (bf16[128,2048]{1,0:T(8,128)(2,1)S(1)}, bf16[128,2048]{1,0:T(8,128)(2,1)}, u32[]{:S(2)}) copy-start(bf16[128,2048]{1,0:T(8,128)(2,1)} %param.21) | copy-start | bytes 1572868
  113.6 8.5 %copy-start.21 = (f32[128]{0:T(128)S(1)}, f32[128]{0:T(128)}, u32[]{:S(2)}) copy-start(f32[128]{0:T(128)} %copy-done.20) | copy-start | bytes 1540
  118.7 11.2 %all-to-all-start.1 = ((bf16[4,32,2048]{2,1,0:T(8,128)(2,1)}), bf16[4,32,2048]{2,1,0:T(8,128)(2,1)S(1)}, u32[]{:S(2)}, u32[]{:S(2)}) async-start(bf16[4,32,2048]{2,1,0:T(8,128)(2,1)} %bitcast.20), calls=%async_computation.1 | async-start | bytes 1048576 | tf_op jit(solution)/shard_map/all_to_all | solution.py:34
  133.0 21.8 %all-to-all-start.2 = ((bf16[32,8,256]{2,0,1:T(8,128)(2,1)}), bf16[32,8,256]{2,0,1:T(8,128)(2,1)S(1)}, u32[]{:S(2)}, u32[]{:S(2)}) async-start(bf16[32,8,256]{2,0,1:T(8,128)(2,1)} %bitcast.53), calls=%async_computation.2 | async-start | bytes 262144 | tf_op jit(solution)/shard_map/all_to_all | solution.py:86
  138.4 155.8 %all-gather.11.cloned.1.call-start = ((), (), s32[]{:S(2)}) async-start(), calls=%async_computation.9 | async-start | bytes 4866048 | tf_op jit(solution)/shard_map/all_gather | solution.py:142
  147.1 53.9 %copy-start.3 = (bf16[128,2048]{1,0:T(8,128)(2,1)}, bf16[128,2048]{1,0:T(8,128)(2,1)S(1)}, u32[]{:S(2)}) copy-start(bf16[128,2048]{1,0:T(8,128)(2,1)S(1)} %all_gather.41) | copy-start | bytes 1572868
  201.0 3.6 %copy-start.19 = (f32[128]{0:T(128)S(1)}, f32[128]{0:T(128)}, u32[]{:S(2)}) copy-start(f32[128]{0:T(128)} %copy-done.18) | copy-start | bytes 1540
  203.8 1.2 copy-start.2
  214.3 11.3 %all-to-all-start.3 = ((bf16[4,32,2048]{2,1,0:T(8,128)(2,1)}), bf16[4,32,2048]{2,1,0:T(8,128)(2,1)S(1)}, u32[]{:S(2)}, u32[]{:S(2)}) async-start(bf16[4,32,2048]{2,1,0:T(8,128)(2,1)} %bitcast.26), calls=%async_computation.3 | async-start | bytes 1048576 | tf_op jit(solution)/shard_map/all_to_all | solution.py:34
  225.6 25.0 %all-to-all-start.5 = ((bf16[4,32,2048]{2,1,0:T(8,128)(2,1)}), bf16[4,32,2048]{2,1,0:T(8,128)(2,1)S(1)}, u32[]{:S(2)}, u32[]{:S(2)}) async-start(bf16[4,32,2048]{2,1,0:T(8,128)(2,1)} %bitcast.72), calls=%async_computation.5 | async-start | bytes 1048576 | tf_op jit(solution)/shard_map/all_to_all | solution.py:34
  250.7 16.3 %all-to-all-start.4 = ((bf16[4,32,2048]{2,1,0:T(8,128)(2,1)}), bf16[4,32,2048]{2,1,0:T(8,128)(2,1)}, u32[]{:S(2)}, u32[]{:S(2)}) async-start(bf16[4,32,2048]{2,1,0:T(8,128)(2,1)} %bitcast.73), calls=%async_computation.4 | async-start | bytes 1048576 | tf_op jit(solution)/shard_map/all_to_all | solution.py:34
  254.9 23.9 %copy-start.7 = (f32[256,704]{0,1:T(8,128)S(1)}, f32[256,704]{0,1:T(8,128)}, u32[]{:S(2)}) copy-start(f32[256,704]{0,1:T(8,128)} %param.34) | copy-start | bytes 2162692
  278.8 2.9 copy-start.8
  278.8 5.8 %copy-start.10 = (bf16[4,8,32,256]{3,2,0,1:T(8,128)(2,1)S(1)}, bf16[4,8,32,256]{3,2,0,1:T(8,128)(2,1)}, u32[]{:S(2)}) copy-start(bf16[4,8,32,256]{3,2,0,1:T(8,128)(2,1)} %copy.90) | copy-start | bytes 1572868
  278.8 5.8 %copy-start.22 = (f32[704,256]{1,0:T(8,128)S(1)}, f32[704,256]{1,0:T(8,128)}, u32[]{:S(2)}) copy-start(f32[704,256]{1,0:T(8,128)} %param.35) | copy-start | bytes 2162692
  281.8 12.5 %copy-start.9 = (f32[256,704]{0,1:T(8,128)S(1)}, f32[256,704]{0,1:T(8,128)}, u32[]{:S(2)}) copy-start(f32[256,704]{0,1:T(8,128)} %param.31) | copy-start | bytes 2162692
  287.4 12.6 %copy-start.11 = (bf16[4,8,32,256]{3,2,0,1:T(8,128)(2,1)S(1)}, bf16[4,8,32,256]{3,2,0,1:T(8,128)(2,1)}, u32[]{:S(2)}) copy-start(bf16[4,8,32,256]{3,2,0,1:T(8,128)(2,1)} %copy.94) | copy-start | bytes 1572868
  294.2 5.8 %copy-start.23 = (f32[704,256]{1,0:T(8,128)S(1)}, f32[704,256]{1,0:T(8,128)}, u32[]{:S(2)}) copy-start(f32[704,256]{1,0:T(8,128)} %param.32) | copy-start | bytes 2162692
  (1 other events, 0.8 us)
Sparse Core Ops, SparseCore 0:
  9.8 95.8 all-gather.6
  107.2 89.2 all-gather.4
  198.7 46.4 all-gather.8
  247.2 46.9 all-gather.10
